TPU v7x, 128 devices: a whole 4x4x4 slice. The times are simulated.
128 devices in a mesh: sp: 16 (over z, y), tp: 8 (over x, core).
Axes of the slice: x: 4, y: 4, z: 4, core: 2. Of those that a mesh axis runs over, the one named last changes fastest.
Arguments:
- residual_in: bfloat16 [12288, 2048], P('sp', 'tp'), may hold values from -11 to 11
- queries: bfloat16 [12288, 1024], P('sp', 'tp'), may hold values from -6 to 6
- keys: bfloat16 [12288, 256], P('sp'), may hold values from -6 to 6
- values: bfloat16 [12288, 256], P('sp'), may hold values from -6 to 6
- query_gain: float32 [128], replicated, may hold values from 1.5 to 5
- key_norm_gain: float32 [128], replicated, may hold values from 1.5 to 5
- out_weight: bfloat16 [1024, 2048], P('tp'), may hold values from -0.1875 to 0.1875
- mlp_gain: float32 [2048], replicated, may hold values from 0.1 to 1.9
- gate_weight: bfloat16 [2048, 5632], P('sp', 'tp'), may hold values from -0.125 to 0.125
- up_weight: bfloat16 [2048, 5632], P('sp', 'tp'), may hold values from -0.125 to 0.125
- down_weight: bfloat16 [5632, 2048], P('tp', 'sp'), may hold values from -0.15625 to 0.15625
Outputs:
- layer_out: bfloat16 [12288, 2048], P('sp', 'tp')
All inputs are finite; a program needn't handle non-finite values.
Results may differ from a plain program's by a relative error of at most 0.012.
The roundings to bfloat16 on the way count: a program that leaves them out, or rounds other values in their place, can miss the bound.
Values may be sent and summed in bfloat16 or wider, within the bound.
A program may use at most 64 MiB of HBM per device.

v0:
```python
import jax
import jax.numpy as jnp
from jax import lax
from jax.sharding import PartitionSpec as P

D = 2048
HEAD_SIZE = 128
QUERY_HEADS = 8
KEY_VALUE_HEADS = 2
GRID = 64
eps = 1e-06
rotary_base = 10000.0


def sent_together(arrays, axis, dim, along):
    ends, at = ([], 0)
    for a in arrays[:-1]:
        at += a.shape[along]
        ends.append(at)
    both = jnp.concatenate(arrays, axis=along)
    return tuple(jnp.split(lax.all_gather(both, axis, axis=dim, tiled=True), ends, axis=along))


def laid_out(tiles, dim):
    tiles = jnp.moveaxis(tiles, 0, dim)
    lengths = tiles.shape
    return tiles.reshape(*lengths[:dim], lengths[dim] * lengths[dim + 1], *lengths[dim + 2 :])


def sent_to_all(x, axis):
    size = lax.axis_size(axis)
    return lax.all_to_all(jnp.broadcast_to(x[None], (size, *x.shape)), axis, 0, 0, tiled=True)


def gathered_copies(x, axis, dim):
    return laid_out(sent_to_all(x, axis), dim)


def taken_together(x, axis):
    everything = sent_to_all(x, axis)
    return jnp.sum(everything, axis=0)


def in_blocks(x, dim, size):
    lengths = x.shape
    tiles = x.reshape(*lengths[:dim], size, lengths[dim] // size, *lengths[dim + 1 :])
    return jnp.moveaxis(tiles, dim, 0)


def summed_on_arrival(x, axis, dim):
    tiles = in_blocks(x, dim, lax.axis_size(axis))
    arrived = lax.all_to_all(tiles, axis, split_axis=0, concat_axis=0, tiled=True)
    return arrived.astype(jnp.float32).sum(axis=0)


def apply_rotary(vectors, grid_positions):
    half_size = vectors.shape[-1] // 2
    frequency = rotary_base ** (-jnp.arange(0, half_size, 2, dtype=jnp.float32) / half_size)
    grid_row = (grid_positions // GRID).astype(jnp.float32)
    grid_col = (grid_positions % GRID).astype(jnp.float32)
    angles = jnp.concatenate(
        [grid_row[:, None] * frequency, grid_col[:, None] * frequency], axis=-1
    )[:, None, :]
    cosine_table = jnp.cos(angles)
    sine_table = jnp.sin(angles)
    first_half = vectors[..., :half_size]
    second_half = vectors[..., half_size:]
    return jnp.concatenate(
        [
            first_half * cosine_table - second_half * sine_table,
            first_half * sine_table + second_half * cosine_table,
        ],
        axis=-1,
    )


def per_head_norm(vectors, gain):
    return vectors * lax.rsqrt(jnp.mean(vectors * vectors, axis=-1, keepdims=True) + eps) * gain


def on_device(
    residual_in,
    queries,
    keys,
    values,
    query_gain,
    key_norm_gain,
    out_weight,
    mlp_gain,
    gate_weight,
    up_weight,
    down_weight,
):
    local_rows = residual_in.shape[0]
    local_heads = queries.shape[1] // HEAD_SIZE
    queries_per_group = QUERY_HEADS // KEY_VALUE_HEADS
    tp_index = lax.axis_index("tp")
    tp_count = lax.axis_size("tp")
    grid_positions = lax.axis_index("sp") * local_rows + jnp.arange(local_rows, dtype=jnp.int32)
    weight_cols = lax.all_to_all(out_weight, "tp", split_axis=1, concat_axis=0, tiled=True)
    query_rows = apply_rotary(
        per_head_norm(
            queries.astype(jnp.float32).reshape(local_rows, local_heads, HEAD_SIZE), query_gain
        ),
        grid_positions,
    ).astype(jnp.bfloat16)
    query_matrix = jnp.transpose(query_rows, (1, 0, 2)).reshape(local_heads * local_rows, HEAD_SIZE)
    shared = tp_index * local_heads // queries_per_group
    own_keys = lax.dynamic_slice_in_dim(keys, shared * HEAD_SIZE, HEAD_SIZE, 1)
    own_values = lax.dynamic_slice_in_dim(values, shared * HEAD_SIZE, HEAD_SIZE, 1)
    key_matrix = apply_rotary(
        per_head_norm(own_keys.astype(jnp.float32)[:, None, :], key_norm_gain), grid_positions
    )[:, 0, :].astype(jnp.bfloat16)
    score_scale = HEAD_SIZE ** (-0.5)
    query_count = local_heads * local_rows
    start_state = (
        jnp.full((query_count,), -1e30, jnp.float32),
        jnp.zeros((query_count,), jnp.float32),
        jnp.zeros((query_count, HEAD_SIZE), jnp.float32),
    )
    key_piece, value_piece = sent_together((key_matrix, own_values), "sp", 0, 1)
    piece_rows = key_piece.shape[0]
    block_count = -(-piece_rows // 2048)
    while piece_rows % block_count:
        block_count += 1
    block_width = piece_rows // block_count

    def one_block(block_index, state_inner):
        running_max, running_sum, weighted = state_inner
        block_keys = lax.dynamic_slice_in_dim(key_piece, block_index * block_width, block_width, 0)
        block_values = lax.dynamic_slice_in_dim(
            value_piece, block_index * block_width, block_width, 0
        )
        scores = (
            jnp.dot(query_matrix, block_keys.T, preferred_element_type=jnp.float32) * score_scale
        )
        new_max = jnp.maximum(running_max, jnp.max(scores, axis=1))
        factor = jnp.exp(running_max - new_max)
        weights = jnp.exp(scores - new_max[:, None])
        running_sum = running_sum * factor + jnp.sum(weights, axis=1)
        weighted = weighted * factor[:, None] + jnp.dot(
            weights.astype(jnp.bfloat16), block_values, preferred_element_type=jnp.float32
        )
        return (new_max, running_sum, weighted)

    running_max, running_sum, weighted = lax.fori_loop(0, block_count, one_block, start_state)
    attended = (weighted / running_sum[:, None]).astype(jnp.bfloat16)
    attended = jnp.transpose(
        attended.reshape(local_heads, local_rows, HEAD_SIZE), (1, 0, 2)
    ).reshape(local_rows, local_heads * HEAD_SIZE)
    own_width = residual_in.shape[1]
    attended_full = gathered_copies(attended, "tp", 1)
    group_width = local_heads * HEAD_SIZE
    share = jnp.zeros((local_rows, own_width), jnp.float32)
    for group_index in range(tp_count):
        left_part = attended_full[:, group_index * group_width : (group_index + 1) * group_width]
        right_part = weight_cols[group_index * group_width : (group_index + 1) * group_width, :]
        term = jnp.dot(left_part, right_part, preferred_element_type=jnp.float32).astype(
            jnp.bfloat16
        )
        share = share + term.astype(jnp.float32)
    residual_mid = residual_in.astype(jnp.float32) + share
    squares = taken_together(jnp.sum(residual_mid * residual_mid, axis=1), "tp")
    gain_own = lax.dynamic_slice_in_dim(mlp_gain, tp_index * own_width, own_width, 0)
    normed_own = (residual_mid * lax.rsqrt(squares / D + eps)[:, None] * gain_own).astype(
        jnp.bfloat16
    )
    normed = lax.all_gather(normed_own, "tp", axis=1, tiled=True)
    pieces = sent_together((gate_weight, up_weight), "sp", 0, 1)
    gate_out = jnp.dot(normed, pieces[0], preferred_element_type=jnp.float32)
    up_out = jnp.dot(normed, pieces[1], preferred_element_type=jnp.float32)
    hidden = (jax.nn.silu(gate_out) * up_out).astype(jnp.bfloat16)
    down_terms = jnp.dot(
        hidden,
        lax.all_gather(down_weight, "sp", axis=1, tiled=True),
        preferred_element_type=jnp.float32,
    )
    down_share = summed_on_arrival(down_terms.astype(jnp.bfloat16), "tp", 1)
    return (residual_mid + 0.5 * down_share).astype(jnp.bfloat16)


def solution(mesh):
    in_specs = (
        P("sp", "tp"),
        P("sp", "tp"),
        P("sp", None),
        P("sp", None),
        P(),
        P(),
        P("tp", None),
        P(),
        P("sp", "tp"),
        P("sp", "tp"),
        P("tp", "sp"),
    )
    out_specs = P("sp", "tp")
    return jax.shard_map(
        on_device, mesh=mesh, in_specs=in_specs, out_specs=out_specs, check_vma=False
    )
```

profile of v0, /device:TPU:1, one launch (start us, length us, event | category | flops | bytes accessed | tf_op | source)
XLA Modules:
  0.0 336.8 jit_solution(7837900333065985362)
XLA Ops:
  14.6 5.8 %all-to-all-start.1 = ((bf16[128,8,256]{0,2,1:T(8,128)(2,1)}), bf16[128,8,256]{0,2,1:T(8,128)(2,1)S(1)}, u32[]{:S(2)}, u32[]{:S(2)}) async-start(bf16[128,8,256]{0,2,1:T(8,128)(2,1)} %bitcast.9), calls=%async_computation.1 | async-start | bytes 1048576 | tf_op jit(solution)/shard_map/all_to_all | solution.py:100
  21.4 56.8 %all-gather.5.cloned.1.call-done = bf16[12288,256]{1,0:T(8,128)(2,1)} async-done(((bf16[768,256]{1,0:T(8,128)(2,1)}), bf16[12288,256]{1,0:T(8,128)(2,1)}) %all-gather.5.cloned.1.call-update) | async-done | bytes 6291472 | tf_op jit(solution)/shard_map/all_gather | solution.py:21
  78.2 4.7 %fusion.66 = (bf16[12288,128]{1,0:T(8,128)(2,1)}, bf16[12288,128]{1,0:T(8,128)(2,1)}) fusion(bf16[12288,256]{1,0:T(8,128)(2,1)} %all-gather.5.cloned.1.call-done), kind=kLoop, calls=%fused_computation.114 | loop fusion | bytes 12582912 | tf_op jit(solution)/shard_map/split | solution.py:21
  82.9 71.6 %while.18 = (s32[]{:T(128)}, f32[768]{0:T(1024)S(1)}, f32[768]{0:T(1024)S(1)}, f32[768,128]{1,0:T(8,128)S(1)}, bf16[12288,128]{1,0:T(8,128)(2,1)}, /*index=5*/bf...) while((s32[]{:T(128)}, f32[768]{0:T(1024)S(1)}, ...), condition=%wide.region_5.6_spmd.clone, body=%wide.region_2.5_spmd.clone.sunk | while | flops 818188032 | bytes 46121160 | solution.py:146
  82.9 4.7 %multiply_reduce_fusion.3 = (f32[768]{0:T(1024)S(1)}, f32[2048,768]{1,0:T(8,128)}) fusion(bf16[768,128]{1,0:T(8,128)(2,1)S(1)} %get-tuple-element.268, bf16[12288,128]{1,0:T(8,128)(2,1)} %get-tuple-element.267, s32[]{:T(128)S(6)} %select_n.55), kind=kOutput, calls=%fused_computation.1.clone.1 | convolution fusion | flops 405798144 | bytes 7015428 | tf_op jit(solution)/shard_map/while/body/eval_jaxpr/dot_general | solution.py:135
  87.6 4.2 %fusion.80 = f32[768]{0:T(1024)S(1)} fusion(f32[2048,768]{1,0:T(8,128)} %get-tuple-element.238, f32[768]{0:T(1024)S(1)} %select_maximum_fusion.2), kind=kLoop, calls=%fused_computation.3.clone.1 | loop fusion | flops 4717824 | bytes 6297600 | tf_op jit(solution)/shard_map/while/body/eval_jaxpr/reduce_sum | solution.py:140
  92.6 2.4 fusion.82
  95.0 4.7 %multiply_reduce_fusion.3 = (f32[768]{0:T(1024)S(1)}, f32[2048,768]{1,0:T(8,128)}) fusion(bf16[768,128]{1,0:T(8,128)(2,1)S(1)} %get-tuple-element.268, bf16[12288,128]{1,0:T(8,128)(2,1)} %get-tuple-element.267, s32[]{:T(128)S(6)} %select_n.55), kind=kOutput, calls=%fused_computation.1.clone.1 | convolution fusion | flops 405798144 | bytes 7015428 | tf_op jit(solution)/shard_map/while/body/eval_jaxpr/dot_general | solution.py:135
  99.6 4.1 %fusion.80 = f32[768]{0:T(1024)S(1)} fusion(f32[2048,768]{1,0:T(8,128)} %get-tuple-element.238, f32[768]{0:T(1024)S(1)} %select_maximum_fusion.2), kind=kLoop, calls=%fused_computation.3.clone.1 | loop fusion | flops 4717824 | bytes 6297600 | tf_op jit(solution)/shard_map/while/body/eval_jaxpr/reduce_sum | solution.py:140
  104.3 2.4 fusion.82
  106.7 4.7 %multiply_reduce_fusion.3 = (f32[768]{0:T(1024)S(1)}, f32[2048,768]{1,0:T(8,128)}) fusion(bf16[768,128]{1,0:T(8,128)(2,1)S(1)} %get-tuple-element.268, bf16[12288,128]{1,0:T(8,128)(2,1)} %get-tuple-element.267, s32[]{:T(128)S(6)} %select_n.55), kind=kOutput, calls=%fused_computation.1.clone.1 | convolution fusion | flops 405798144 | bytes 7015428 | tf_op jit(solution)/shard_map/while/body/eval_jaxpr/dot_general | solution.py:135
  111.4 4.2 %fusion.80 = f32[768]{0:T(1024)S(1)} fusion(f32[2048,768]{1,0:T(8,128)} %get-tuple-element.238, f32[768]{0:T(1024)S(1)} %select_maximum_fusion.2), kind=kLoop, calls=%fused_computation.3.clone.1 | loop fusion | flops 4717824 | bytes 6297600 | tf_op jit(solution)/shard_map/while/body/eval_jaxpr/reduce_sum | solution.py:140
  116.4 2.4 fusion.82
  118.8 4.7 %multiply_reduce_fusion.3 = (f32[768]{0:T(1024)S(1)}, f32[2048,768]{1,0:T(8,128)}) fusion(bf16[768,128]{1,0:T(8,128)(2,1)S(1)} %get-tuple-element.268, bf16[12288,128]{1,0:T(8,128)(2,1)} %get-tuple-element.267, s32[]{:T(128)S(6)} %select_n.55), kind=kOutput, calls=%fused_computation.1.clone.1 | convolution fusion | flops 405798144 | bytes 7015428 | tf_op jit(solution)/shard_map/while/body/eval_jaxpr/dot_general | solution.py:135
  123.5 4.2 %fusion.80 = f32[768]{0:T(1024)S(1)} fusion(f32[2048,768]{1,0:T(8,128)} %get-tuple-element.238, f32[768]{0:T(1024)S(1)} %select_maximum_fusion.2), kind=kLoop, calls=%fused_computation.3.clone.1 | loop fusion | flops 4717824 | bytes 6297600 | tf_op jit(solution)/shard_map/while/body/eval_jaxpr/reduce_sum | solution.py:140
  128.5 2.4 fusion.82
  130.9 4.7 %multiply_reduce_fusion.3 = (f32[768]{0:T(1024)S(1)}, f32[2048,768]{1,0:T(8,128)}) fusion(bf16[768,128]{1,0:T(8,128)(2,1)S(1)} %get-tuple-element.268, bf16[12288,128]{1,0:T(8,128)(2,1)} %get-tuple-element.267, s32[]{:T(128)S(6)} %select_n.55), kind=kOutput, calls=%fused_computation.1.clone.1 | convolution fusion | flops 405798144 | bytes 7015428 | tf_op jit(solution)/shard_map/while/body/eval_jaxpr/dot_general | solution.py:135
  135.6 4.2 %fusion.80 = f32[768]{0:T(1024)S(1)} fusion(f32[2048,768]{1,0:T(8,128)} %get-tuple-element.238, f32[768]{0:T(1024)S(1)} %select_maximum_fusion.2), kind=kLoop, calls=%fused_computation.3.clone.1 | loop fusion | flops 4717824 | bytes 6297600 | tf_op jit(solution)/shard_map/while/body/eval_jaxpr/reduce_sum | solution.py:140
  140.5 2.4 fusion.82
  142.9 4.7 %multiply_reduce_fusion.3 = (f32[768]{0:T(1024)S(1)}, f32[2048,768]{1,0:T(8,128)}) fusion(bf16[768,128]{1,0:T(8,128)(2,1)S(1)} %get-tuple-element.268, bf16[12288,128]{1,0:T(8,128)(2,1)} %get-tuple-element.267, s32[]{:T(128)S(6)} %select_n.55), kind=kOutput, calls=%fused_computation.1.clone.1 | convolution fusion | flops 405798144 | bytes 7015428 | tf_op jit(solution)/shard_map/while/body/eval_jaxpr/dot_general | solution.py:135
  147.5 4.0 %fusion.80 = f32[768]{0:T(1024)S(1)} fusion(f32[2048,768]{1,0:T(8,128)} %get-tuple-element.238, f32[768]{0:T(1024)S(1)} %select_maximum_fusion.2), kind=kLoop, calls=%fused_computation.3.clone.1 | loop fusion | flops 4717824 | bytes 6297600 | tf_op jit(solution)/shard_map/while/body/eval_jaxpr/reduce_sum | solution.py:140
  152.1 2.4 fusion.82
  156.2 5.2 %all-to-all-start = ((bf16[8,768,128]{1,2,0:T(8,128)(2,1)}), bf16[8,768,128]{1,2,0:T(8,128)(2,1)S(1)}, u32[]{:S(2)}, u32[]{:S(2)}) async-start(bf16[8,768,128]{1,2,0:T(8,128)(2,1)} %broadcast_in_dim.17), calls=%async_computation | async-start | bytes 3145728 | tf_op jit(solution)/shard_map/all_to_all | solution.py:32
  163.3 18.7 %all-to-all-done = bf16[8,768,128]{1,2,0:T(8,128)(2,1)S(1)} async-done(((bf16[8,768,128]{1,2,0:T(8,128)(2,1)}), bf16[8,768,128]{1,2,0:T(8,128)(2,1)S(1)}, u32[]{:S(2)}, u32[]{:S(2)}) %all-to-all-start) | async-done | bytes 1572896 | tf_op jit(solution)/shard_map/all_to_all | solution.py:32
  184.9 4.2 %all-to-all-start.2 = ((f32[8,1,768]{2,1,0:T(1,128)}), f32[8,1,768]{2,1,0:T(1,128)S(1)}, u32[]{:S(2)}, u32[]{:S(2)}) async-start(f32[8,1,768]{2,1,0:T(1,128)} %broadcast_in_dim.18), calls=%async_computation.2 | async-start | bytes 49152 | tf_op jit(solution)/shard_map/all_to_all | solution.py:32
  189.9 3.9 %all-to-all-done.2 = f32[8,1,768]{2,1,0:T(1,128)S(1)} async-done(((f32[8,1,768]{2,1,0:T(1,128)}), f32[8,1,768]{2,1,0:T(1,128)S(1)}, u32[]{:S(2)}, u32[]{:S(2)}) %all-to-all-start.2) | async-done | bytes 24608 | tf_op jit(solution)/shard_map/all_to_all | solution.py:32
  195.3 24.9 %all-gather.7.cloned.1.call-done = bf16[768,2048]{0,1:T(8,128)(2,1)} async-done(((bf16[768,256]{0,1:T(8,128)(2,1)}), bf16[768,2048]{0,1:T(8,128)(2,1)}) %all-gather.7.cloned.1.call-update) | async-done | bytes 3145744 | tf_op jit(solution)/shard_map/all_gather | solution.py:168
  220.2 5.2 %fusion.16 = f32[768,704]{0,1:T(8,128)S(1)} fusion(bf16[768,2048]{0,1:T(8,128)(2,1)} %all-gather.7.cloned.1.call-done, bf16[2048,1408]{0,1:T(8,128)(2,1)} %all-gather.9.cloned.1.call-done), kind=kOutput, calls=%fused_computation.22 | convolution fusion | flops 2214592512 | bytes 8192000 | tf_op jit(solution)/shard_map/dot_general | solution.py:170
  225.4 45.8 %all-gather.11.cloned.1.call-done = bf16[704,2048]{1,0:T(8,128)(2,1)} async-done(((bf16[704,128]{1,0:T(8,128)(2,1)}), bf16[704,2048]{1,0:T(8,128)(2,1)}) %all-gather.11.cloned.1.call-update) | async-done | bytes 2883600 | tf_op jit(solution)/shard_map/all_gather | solution.py:175
  271.2 11.7 %convolution_convert_fusion = bf16[768,2048]{1,0:T(8,128)(2,1)} fusion(bf16[704,2048]{1,0:T(8,128)(2,1)} %all-gather.11.cloned.1.call-done, f32[768,704]{0,1:T(8,128)S(1)} %fusion.16, bf16[768,2048]{0,1:T(8,128)(2,1)} %all-gather.7.cloned.1.call-done, bf16[2048,1408]{0,1:T(8,128)(2,1)} %all-gather.9.cloned.1.call-done), kind=kOutput, calls=%fused_computation.18 | convolution fusion | flops 4434001920 | bytes 14221312 | tf_op jit(solution)/shard_map/dot_general | solution.py:173
  282.9 2.1 copy.79
  285.0 43.5 %all_to_all.32 = bf16[8,768,256]{2,1,0:T(8,128)(2,1)S(1)} all-to-all(bf16[8,768,256]{2,1,0:T(8,128)(2,1)S(1)} %bitcast.66), channel_id=1, replica_groups=mesh['sp'=16,'tp'=8] {'tp'}, dimensions={0} | all-to-all | bytes 6291456 | tf_op jit(solution)/shard_map/all_to_all | solution.py:52
  (90 shorter events, 23.5 us)
Async XLA Ops:
  6.5 2.4 copy-start
  6.5 71.7 %all-gather.5.cloned.1.call-start = ((), (), s32[]{:S(2)}) async-start(), calls=%async_computation.4 | async-start | bytes 6684672 | tf_op jit(solution)/shard_map/all_gather | solution.py:21
  10.5 3.1 copy-start.3
  12.3 8.1 %copy-start.4 = (bf16[128,704]{0,1:T(8,128)(2,1)S(1)}, bf16[128,704]{0,1:T(8,128)(2,1)}, u32[]{:S(2)}) copy-start(bf16[128,704]{0,1:T(8,128)(2,1)} %param.22) | copy-start | bytes 540676
  12.3 8.1 %copy-start.5 = (bf16[128,704]{0,1:T(8,128)(2,1)S(1)}, bf16[128,704]{0,1:T(8,128)(2,1)}, u32[]{:S(2)}) copy-start(bf16[128,704]{0,1:T(8,128)(2,1)} %param.21) | copy-start | bytes 540676
  14.6 140.2 %all-to-all-start.1 = ((bf16[128,8,256]{0,2,1:T(8,128)(2,1)}), bf16[128,8,256]{0,2,1:T(8,128)(2,1)S(1)}, u32[]{:S(2)}, u32[]{:S(2)}) async-start(bf16[128,8,256]{0,2,1:T(8,128)(2,1)} %bitcast.9), calls=%async_computation.1 | async-start | bytes 1048576 | tf_op jit(solution)/shard_map/all_to_all | solution.py:100
  20.4 174.9 %all-gather.9.cloned.1.call-start = ((), (), s32[]{:S(2)}) async-start(), calls=%async_computation.6 | async-start | bytes 6127616 | tf_op jit(solution)/shard_map/all_gather | solution.py:21
  87.6 5.0 %copy-start.1 = (f32[2048,768]{1,0:T(8,128)S(1)}, f32[2048,768]{1,0:T(8,128)}, u32[]{:S(2)}) copy-start(f32[2048,768]{1,0:T(8,128)} %get-tuple-element.238) | copy-start | bytes 18874372 | tf_op jit(solution)/shard_map/while
  99.6 4.7 %copy-start.1 = (f32[2048,768]{1,0:T(8,128)S(1)}, f32[2048,768]{1,0:T(8,128)}, u32[]{:S(2)}) copy-start(f32[2048,768]{1,0:T(8,128)} %get-tuple-element.238) | copy-start | bytes 18874372 | tf_op jit(solution)/shard_map/while
  111.4 5.0 %copy-start.1 = (f32[2048,768]{1,0:T(8,128)S(1)}, f32[2048,768]{1,0:T(8,128)}, u32[]{:S(2)}) copy-start(f32[2048,768]{1,0:T(8,128)} %get-tuple-element.238) | copy-start | bytes 18874372 | tf_op jit(solution)/shard_map/while
  123.5 5.0 %copy-start.1 = (f32[2048,768]{1,0:T(8,128)S(1)}, f32[2048,768]{1,0:T(8,128)}, u32[]{:S(2)}) copy-start(f32[2048,768]{1,0:T(8,128)} %get-tuple-element.238) | copy-start | bytes 18874372 | tf_op jit(solution)/shard_map/while
  135.6 4.9 %copy-start.1 = (f32[2048,768]{1,0:T(8,128)S(1)}, f32[2048,768]{1,0:T(8,128)}, u32[]{:S(2)}) copy-start(f32[2048,768]{1,0:T(8,128)} %get-tuple-element.238) | copy-start | bytes 18874372 | tf_op jit(solution)/shard_map/while
  147.5 4.6 %copy-start.1 = (f32[2048,768]{1,0:T(8,128)S(1)}, f32[2048,768]{1,0:T(8,128)}, u32[]{:S(2)}) copy-start(f32[2048,768]{1,0:T(8,128)} %get-tuple-element.238) | copy-start | bytes 18874372 | tf_op jit(solution)/shard_map/while
  156.2 25.8 %all-to-all-start = ((bf16[8,768,128]{1,2,0:T(8,128)(2,1)}), bf16[8,768,128]{1,2,0:T(8,128)(2,1)S(1)}, u32[]{:S(2)}, u32[]{:S(2)}) async-start(bf16[8,768,128]{1,2,0:T(8,128)(2,1)} %broadcast_in_dim.17), calls=%async_computation | async-start | bytes 3145728 | tf_op jit(solution)/shard_map/all_to_all | solution.py:32
  183.0 1.0 copy-start.2
  184.9 8.9 %all-to-all-start.2 = ((f32[8,1,768]{2,1,0:T(1,128)}), f32[8,1,768]{2,1,0:T(1,128)S(1)}, u32[]{:S(2)}, u32[]{:S(2)}) async-start(f32[8,1,768]{2,1,0:T(1,128)} %broadcast_in_dim.18), calls=%async_computation.2 | async-start | bytes 49152 | tf_op jit(solution)/shard_map/all_to_all | solution.py:32
  189.1 31.1 %all-gather.7.cloned.1.call-start = ((), (), s32[]{:S(2)}) async-start(), calls=%async_computation.5 | async-start | bytes 3538944 | tf_op jit(solution)/shard_map/all_gather | solution.py:168
  194.7 76.4 %all-gather.11.cloned.1.call-start = ((), (), s32[]{:S(2)}) async-start(), calls=%async_computation.7 | async-start | bytes 3063808 | tf_op jit(solution)/shard_map/all_gather | solution.py:175
Sparse Core Ops, SparseCore 0:
  13.7 64.4 all-gather.4
  80.3 62.8 all-gather.8
  194.9 25.3 all-gather.6
  222.2 48.9 all-gather.10
where the time goes:
time: 338 us; the launch traced here: 337 us
  waiting for transfers between devices  151 us (45%)
  matrix products  61.1 us (18%)
  blocking collectives  43.5 us (13%)
  other arithmetic  34.3 us (10%)
  local copies, waits for them, and re-layouts  18.2 us (5%)
  starting transfers between devices  15.5 us (5%)
  between operations  13.4 us (4%)
    all_gather x2, waiting for transfers between devices, sent_together(): lax.all_gather(both, axis, axis=dim, tiled=True)  56.8 us
    all_gather x1, waiting for transfers between devices, on_device(): lax.all_gather(down_weight, 'sp', axis=1, tiled=True)  45.8 us
    all_to_all x1, blocking collectives, summed_on_arrival(): lax.all_to_all(tiles, axis, split_axis=0, concat_axis=0, tiled=True)  43.5 us
    dot_general x6, matrix products, one_block(): jnp.dot(query_matrix, block_keys.T, preferred_element_type=jnp.float32)  28 us
    all_gather x1, waiting for transfers between devices, on_device(): normed = lax.all_gather(normed_own, 'tp', axis=1, tiled=True)  24.9 us
    reduce_sum x6, other arithmetic, one_block(): running_sum = running_sum * factor + jnp.sum(weights, axis=1)  24.8 us
    all_to_all x2, waiting for transfers between devices, sent_to_all(): lax.all_to_all(jnp.broadcast_to(x[None], (size, *x.shape)), axis, 0, 0, t...  22.6 us
    dot_general x6, matrix products, one_block(): jnp.dot(weights.astype(jnp.bfloat16), block_values, preferred_element_typ...  14.2 us
  transfers between devices with their start and end apart: 7, of which 5 were waited for; matrix products, arithmetic and copies ran while one was open for 26% of the time, Pallas kernels for 0%

commit v1 on v0

--- a/solution.py
+++ b/solution.py
@@ -2,6 +2,7 @@
 import jax.numpy as jnp
 from jax import lax
 from jax.sharding import PartitionSpec as P
+from jax.lax import all_to_all, axis_size
 
 D = 2048
 HEAD_SIZE = 128
@@ -91,6 +92,17 @@
     up_weight,
     down_weight,
 ):
+
+    def produce_leaves_here(patch):
+        n_peers_all = axis_size("tp")
+        return all_to_all(
+            jnp.tile(patch, [n_peers_all if rr == 1 else 1 for rr in range(patch.ndim)]),
+            axis_name="tp",
+            split_axis=1,
+            concat_axis=1,
+            tiled=True,
+        )
+
     local_rows = residual_in.shape[0]
     local_heads = queries.shape[1] // HEAD_SIZE
     queries_per_group = QUERY_HEADS // KEY_VALUE_HEADS
@@ -165,7 +177,7 @@
     normed_own = (residual_mid * lax.rsqrt(squares / D + eps)[:, None] * gain_own).astype(
         jnp.bfloat16
     )
-    normed = lax.all_gather(normed_own, "tp", axis=1, tiled=True)
+    normed = produce_leaves_here(normed_own)
     pieces = sent_together((gate_weight, up_weight), "sp", 0, 1)
     gate_out = jnp.dot(normed, pieces[0], preferred_element_type=jnp.float32)
     up_out = jnp.dot(normed, pieces[1], preferred_element_type=jnp.float32)

time: 338 us -> 308 us (0.911)
  waiting for transfers between devices: 151 us -> 80.5 us
  blocking collectives: 43.5 us -> 81.6 us
    all_gather x1, waiting for transfers between devices: 45.8 us -> 0.01 us  [on_device(): lax.all_gather(down_weight, 'sp', axis=1, tiled=True)]
    all_to_all x0 -> x1, blocking collectives: none -> 40.5 us  [produce_leaves_here(): all_to_all(jnp.tile(patch, [n_peers_all if rr == 1 else 1 for rr in range...]
    all_gather x1 -> x0, waiting for transfers between devices: 24.9 us -> none  [on_device(): normed = lax.all_gather(normed_own, 'tp', axis=1, tiled=True)]
    dot_general x8, matrix products: 1.99 us -> 8.71 us  [on_device(): jnp.dot(left_part, right_part, preferred_element_type=jnp.float32)]
    dot_general x6, matrix products: 14.2 us -> 7.94 us  [one_block(): jnp.dot(weights.astype(jnp.bfloat16), block_values, preferred_element_typ...]
  transfers between devices with their start and end apart: 7 -> 6, of which waited for: 5 -> 3; matrix products, arithmetic and copies ran while one was open for 26% -> 29% of each run, Pallas kernels for 0% -> 0%
where the time goes in v1:
time: 308 us; the launch traced here: 307 us
  blocking collectives  81.6 us (26%)
  waiting for transfers between devices  80.5 us (26%)
  matrix products  63.2 us (21%)
  other arithmetic  33.7 us (11%)
  local copies, waits for them, and re-layouts  19 us (6%)
  starting transfers between devices  15.1 us (5%)
  between operations  13.4 us (4%)
    all_gather x2, waiting for transfers between devices, sent_together(): lax.all_gather(both, axis, axis=dim, tiled=True)  56.1 us
    all_to_all x1, blocking collectives, summed_on_arrival(): lax.all_to_all(tiles, axis, split_axis=0, concat_axis=0, tiled=True)  41 us
    all_to_all x1, blocking collectives, produce_leaves_here(): all_to_all(jnp.tile(patch, [n_peers_all if rr == 1 else 1 for rr in range...  40.5 us
    dot_general x6, matrix products, one_block(): jnp.dot(query_matrix, block_keys.T, preferred_element_type=jnp.float32)  28.4 us
    reduce_sum x6, other arithmetic, one_block(): running_sum = running_sum * factor + jnp.sum(weights, axis=1)  24.2 us
    all_to_all x2, waiting for transfers between devices, sent_to_all(): lax.all_to_all(jnp.broadcast_to(x[None], (size, *x.shape)), axis, 0, 0, t...  23.7 us
    dot_general x1, matrix products, on_device(): jnp.dot(hidden, lax.all_gather(down_weight, 'sp', axis=1, tiled=True), pr...  11.5 us
    all_to_all x2, starting transfers between devices, sent_to_all(): lax.all_to_all(jnp.broadcast_to(x[None], (size, *x.shape)), axis, 0, 0, t...  9.3 us
  transfers between devices with their start and end apart: 6, of which 3 were waited for; matrix products, arithmetic and copies ran while one was open for 29% of the time, Pallas kernels for 0%

profile of v1, /device:TPU:1, one launch (start us, length us, event | category | flops | bytes accessed | tf_op | source)
XLA Modules:
  0.0 306.6 jit_solution(2725025384899518010)
XLA Ops:
  9.2 1.3 fusion.40
  10.5 1.8 fusion.44
  14.7 5.8 %all-to-all-start.1 = ((bf16[128,8,256]{0,2,1:T(8,128)(2,1)}), bf16[128,8,256]{0,2,1:T(8,128)(2,1)}, u32[]{:S(2)}, u32[]{:S(2)}) async-start(bf16[128,8,256]{0,2,1:T(8,128)(2,1)} %bitcast.9), calls=%async_computation.1 | async-start | bytes 1048576 | tf_op jit(solution)/shard_map/all_to_all | solution.py:112
  22.1 56.1 %all-gather.4.cloned.1.call-done = bf16[12288,256]{1,0:T(8,128)(2,1)} async-done(((bf16[768,256]{1,0:T(8,128)(2,1)}), bf16[12288,256]{1,0:T(8,128)(2,1)}) %all-gather.4.cloned.1.call-update) | async-done | bytes 6291472 | tf_op jit(solution)/shard_map/all_gather | solution.py:22
  78.2 4.2 %fusion.66 = (bf16[12288,128]{1,0:T(8,128)(2,1)S(1)}, bf16[12288,128]{1,0:T(8,128)(2,1)}) fusion(bf16[12288,256]{1,0:T(8,128)(2,1)} %all-gather.4.cloned.1.call-done), kind=kLoop, calls=%fused_computation.114 | loop fusion | bytes 12582912 | tf_op jit(solution)/shard_map/split | solution.py:22
  82.4 64.6 %while.18 = (s32[]{:T(128)}, f32[768]{0:T(1024)S(1)}, f32[768]{0:T(1024)S(1)}, f32[768,128]{1,0:T(8,128)S(1)}, bf16[12288,128]{1,0:T(8,128)(2,1)}, /*index=5*/bf...) while((s32[]{:T(128)}, f32[768]{0:T(1024)S(1)}, ...), condition=%wide.region_5.6_spmd.clone, body=%wide.region_2.5_spmd.clone.sunk | while | flops 818188032 | bytes 46123208 | solution.py:158
  82.4 4.7 %multiply_reduce_fusion.3 = (f32[768]{0:T(1024)S(1)}, f32[2048,768]{1,0:T(8,128)}) fusion(bf16[768,128]{1,0:T(8,128)(2,1)} %get-tuple-element.268, bf16[12288,128]{1,0:T(8,128)(2,1)} %get-tuple-element.267, s32[]{:T(128)S(6)} %select_n.55), kind=kOutput, calls=%fused_computation.1.clone.1 | convolution fusion | flops 405798144 | bytes 7015428 | tf_op jit(solution)/shard_map/while/body/eval_jaxpr/dot_general | solution.py:147
  87.1 4.1 %fusion.80 = f32[768]{0:T(1024)S(1)} fusion(f32[2048,768]{1,0:T(8,128)} %get-tuple-element.238, f32[768]{0:T(1024)S(1)} %select_maximum_fusion.2), kind=kLoop, calls=%fused_computation.3.clone.1 | loop fusion | flops 4717824 | bytes 6297600 | tf_op jit(solution)/shard_map/while/body/eval_jaxpr/reduce_sum | solution.py:152
  92.0 1.3 fusion.82
  93.4 4.7 %multiply_reduce_fusion.3 = (f32[768]{0:T(1024)S(1)}, f32[2048,768]{1,0:T(8,128)}) fusion(bf16[768,128]{1,0:T(8,128)(2,1)} %get-tuple-element.268, bf16[12288,128]{1,0:T(8,128)(2,1)} %get-tuple-element.267, s32[]{:T(128)S(6)} %select_n.55), kind=kOutput, calls=%fused_computation.1.clone.1 | convolution fusion | flops 405798144 | bytes 7015428 | tf_op jit(solution)/shard_map/while/body/eval_jaxpr/dot_general | solution.py:147
  98.1 4.1 %fusion.80 = f32[768]{0:T(1024)S(1)} fusion(f32[2048,768]{1,0:T(8,128)} %get-tuple-element.238, f32[768]{0:T(1024)S(1)} %select_maximum_fusion.2), kind=kLoop, calls=%fused_computation.3.clone.1 | loop fusion | flops 4717824 | bytes 6297600 | tf_op jit(solution)/shard_map/while/body/eval_jaxpr/reduce_sum | solution.py:152
  102.8 1.3 fusion.82
  104.1 4.7 %multiply_reduce_fusion.3 = (f32[768]{0:T(1024)S(1)}, f32[2048,768]{1,0:T(8,128)}) fusion(bf16[768,128]{1,0:T(8,128)(2,1)} %get-tuple-element.268, bf16[12288,128]{1,0:T(8,128)(2,1)} %get-tuple-element.267, s32[]{:T(128)S(6)} %select_n.55), kind=kOutput, calls=%fused_computation.1.clone.1 | convolution fusion | flops 405798144 | bytes 7015428 | tf_op jit(solution)/shard_map/while/body/eval_jaxpr/dot_general | solution.py:147
  108.9 4.0 %fusion.80 = f32[768]{0:T(1024)S(1)} fusion(f32[2048,768]{1,0:T(8,128)} %get-tuple-element.238, f32[768]{0:T(1024)S(1)} %select_maximum_fusion.2), kind=kLoop, calls=%fused_computation.3.clone.1 | loop fusion | flops 4717824 | bytes 6297600 | tf_op jit(solution)/shard_map/while/body/eval_jaxpr/reduce_sum | solution.py:152
  113.5 1.3 fusion.82
  114.8 4.7 %multiply_reduce_fusion.3 = (f32[768]{0:T(1024)S(1)}, f32[2048,768]{1,0:T(8,128)}) fusion(bf16[768,128]{1,0:T(8,128)(2,1)} %get-tuple-element.268, bf16[12288,128]{1,0:T(8,128)(2,1)} %get-tuple-element.267, s32[]{:T(128)S(6)} %select_n.55), kind=kOutput, calls=%fused_computation.1.clone.1 | convolution fusion | flops 405798144 | bytes 7015428 | tf_op jit(solution)/shard_map/while/body/eval_jaxpr/dot_general | solution.py:147
  119.6 4.0 %fusion.80 = f32[768]{0:T(1024)S(1)} fusion(f32[2048,768]{1,0:T(8,128)} %get-tuple-element.238, f32[768]{0:T(1024)S(1)} %select_maximum_fusion.2), kind=kLoop, calls=%fused_computation.3.clone.1 | loop fusion | flops 4717824 | bytes 6297600 | tf_op jit(solution)/shard_map/while/body/eval_jaxpr/reduce_sum | solution.py:152
  125.5 4.7 %multiply_reduce_fusion.3 = (f32[768]{0:T(1024)S(1)}, f32[2048,768]{1,0:T(8,128)}) fusion(bf16[768,128]{1,0:T(8,128)(2,1)} %get-tuple-element.268, bf16[12288,128]{1,0:T(8,128)(2,1)} %get-tuple-element.267, s32[]{:T(128)S(6)} %select_n.55), kind=kOutput, calls=%fused_computation.1.clone.1 | convolution fusion | flops 405798144 | bytes 7015428 | tf_op jit(solution)/shard_map/while/body/eval_jaxpr/dot_general | solution.py:147
  130.3 4.0 %fusion.80 = f32[768]{0:T(1024)S(1)} fusion(f32[2048,768]{1,0:T(8,128)} %get-tuple-element.238, f32[768]{0:T(1024)S(1)} %select_maximum_fusion.2), kind=kLoop, calls=%fused_computation.3.clone.1 | loop fusion | flops 4717824 | bytes 6297600 | tf_op jit(solution)/shard_map/while/body/eval_jaxpr/reduce_sum | solution.py:152
  134.9 1.3 fusion.82
  136.3 4.7 %multiply_reduce_fusion.3 = (f32[768]{0:T(1024)S(1)}, f32[2048,768]{1,0:T(8,128)}) fusion(bf16[768,128]{1,0:T(8,128)(2,1)} %get-tuple-element.268, bf16[12288,128]{1,0:T(8,128)(2,1)} %get-tuple-element.267, s32[]{:T(128)S(6)} %select_n.55), kind=kOutput, calls=%fused_computation.1.clone.1 | convolution fusion | flops 405798144 | bytes 7015428 | tf_op jit(solution)/shard_map/while/body/eval_jaxpr/dot_general | solution.py:147
  141.0 4.0 %fusion.80 = f32[768]{0:T(1024)S(1)} fusion(f32[2048,768]{1,0:T(8,128)} %get-tuple-element.238, f32[768]{0:T(1024)S(1)} %select_maximum_fusion.2), kind=kLoop, calls=%fused_computation.3.clone.1 | loop fusion | flops 4717824 | bytes 6297600 | tf_op jit(solution)/shard_map/while/body/eval_jaxpr/reduce_sum | solution.py:152
  148.6 5.1 %all-to-all-start = ((bf16[8,768,128]{1,2,0:T(8,128)(2,1)}), bf16[8,768,128]{1,2,0:T(8,128)(2,1)S(1)}, u32[]{:S(2)}, u32[]{:S(2)}) async-start(bf16[8,768,128]{1,2,0:T(8,128)(2,1)} %broadcast_in_dim.17), calls=%async_computation | async-start | bytes 3145728 | tf_op jit(solution)/shard_map/all_to_all | solution.py:33
  154.6 19.7 %all-to-all-done = bf16[8,768,128]{1,2,0:T(8,128)(2,1)S(1)} async-done(((bf16[8,768,128]{1,2,0:T(8,128)(2,1)}), bf16[8,768,128]{1,2,0:T(8,128)(2,1)S(1)}, u32[]{:S(2)}, u32[]{:S(2)}) %all-to-all-start) | async-done | bytes 1572896 | tf_op jit(solution)/shard_map/all_to_all | solution.py:33
  183.7 4.2 %all-to-all-start.2 = ((f32[8,1,768]{2,1,0:T(1,128)}), f32[8,1,768]{2,1,0:T(1,128)S(1)}, u32[]{:S(2)}, u32[]{:S(2)}) async-start(f32[8,1,768]{2,1,0:T(1,128)} %broadcast_in_dim.18), calls=%async_computation.2 | async-start | bytes 49152 | tf_op jit(solution)/shard_map/all_to_all | solution.py:33
  188.7 4.0 %all-to-all-done.2 = f32[8,1,768]{2,1,0:T(1,128)S(1)} async-done(((f32[8,1,768]{2,1,0:T(1,128)}), f32[8,1,768]{2,1,0:T(1,128)S(1)}, u32[]{:S(2)}, u32[]{:S(2)}) %all-to-all-start.2) | async-done | bytes 24608 | tf_op jit(solution)/shard_map/all_to_all | solution.py:33
  193.3 40.5 %all_to_all.41 = bf16[768,8,256]{2,0,1:T(8,128)(2,1)S(1)} all-to-all(bf16[768,8,256]{2,0,1:T(8,128)(2,1)S(1)} %tile.2), channel_id=1, replica_groups=mesh['sp'=16,'tp'=8] {'tp'}, dimensions={1} | all-to-all | bytes 6291456 | tf_op jit(solution)/shard_map/all_to_all | solution.py:98
  233.8 2.8 copy.95
  236.7 6.7 %fusion.16 = f32[768,704]{0,1:T(8,128)} fusion(bf16[768,2048]{0,1:T(8,128)(2,1)} %bitcast.76, bf16[2048,1408]{0,1:T(8,128)(2,1)} %all-gather.6.cloned.1.call-done), kind=kOutput, calls=%fused_computation.22 | convolution fusion | flops 2214592512 | bytes 8192000 | tf_op jit(solution)/shard_map/dot_general | solution.py:182
  243.4 11.5 %convolution_convert_fusion = bf16[768,2048]{1,0:T(8,128)(2,1)} fusion(bf16[704,2048]{1,0:T(8,128)(2,1)} %all-gather.8.cloned.1.call-done, f32[768,704]{0,1:T(8,128)} %fusion.16, bf16[768,2048]{0,1:T(8,128)(2,1)S(1)} %bitcast.77, bf16[2048,1408]{0,1:T(8,128)(2,1)} %all-gather.6.cloned.1.call-done), kind=kOutput, calls=%fused_computation.18 | convolution fusion | flops 4434001920 | bytes 14221312 | tf_op jit(solution)/shard_map/dot_general | solution.py:185
  254.8 2.1 copy.104
  256.9 41.0 %all_to_all.42 = bf16[8,768,256]{2,1,0:T(8,128)(2,1)S(1)} all-to-all(bf16[8,768,256]{2,1,0:T(8,128)(2,1)S(1)} %bitcast.67), channel_id=1, replica_groups=mesh['sp'=16,'tp'=8] {'tp'}, dimensions={0} | all-to-all | bytes 6291456 | tf_op jit(solution)/shard_map/all_to_all | solution.py:53
  (99 shorter events, 28.3 us)
Async XLA Ops:
  6.5 2.4 copy-start
  6.5 71.7 %all-gather.4.cloned.1.call-start = ((), (), s32[]{:S(2)}) async-start(), calls=%async_computation.5 | async-start | bytes 6684672 | tf_op jit(solution)/shard_map/all_gather | solution.py:22
  10.5 3.1 %copy-start.6 = (bf16[128,2048]{1,0:T(8,128)(2,1)S(1)}, bf16[128,2048]{1,0:T(8,128)(2,1)}, u32[]{:S(2)}) copy-start(bf16[128,2048]{1,0:T(8,128)(2,1)} %param.19) | copy-start | bytes 1572868
  12.3 8.1 %copy-start.8 = (bf16[128,704]{0,1:T(8,128)(2,1)S(1)}, bf16[128,704]{0,1:T(8,128)(2,1)}, u32[]{:S(2)}) copy-start(bf16[128,704]{0,1:T(8,128)(2,1)} %param.22) | copy-start | bytes 540676
  12.3 8.1 %copy-start.9 = (bf16[128,704]{0,1:T(8,128)(2,1)S(1)}, bf16[128,704]{0,1:T(8,128)(2,1)}, u32[]{:S(2)}) copy-start(bf16[128,704]{0,1:T(8,128)(2,1)} %param.21) | copy-start | bytes 540676
  14.7 132.7 %all-to-all-start.1 = ((bf16[128,8,256]{0,2,1:T(8,128)(2,1)}), bf16[128,8,256]{0,2,1:T(8,128)(2,1)}, u32[]{:S(2)}, u32[]{:S(2)}) async-start(bf16[128,8,256]{0,2,1:T(8,128)(2,1)} %bitcast.9), calls=%async_computation.1 | async-start | bytes 1048576 | tf_op jit(solution)/shard_map/all_to_all | solution.py:112
  20.5 216.2 %all-gather.6.cloned.1.call-start = ((), (), s32[]{:S(2)}) async-start(), calls=%async_computation.6 | async-start | bytes 6127616 | tf_op jit(solution)/shard_map/all_gather | solution.py:22
  87.1 4.9 %copy-start.2 = (f32[2048,768]{1,0:T(8,128)S(1)}, f32[2048,768]{1,0:T(8,128)}, u32[]{:S(2)}) copy-start(f32[2048,768]{1,0:T(8,128)} %get-tuple-element.238) | copy-start | bytes 18874372 | tf_op jit(solution)/shard_map/while
  98.1 4.7 %copy-start.2 = (f32[2048,768]{1,0:T(8,128)S(1)}, f32[2048,768]{1,0:T(8,128)}, u32[]{:S(2)}) copy-start(f32[2048,768]{1,0:T(8,128)} %get-tuple-element.238) | copy-start | bytes 18874372 | tf_op jit(solution)/shard_map/while
  108.9 4.6 %copy-start.2 = (f32[2048,768]{1,0:T(8,128)S(1)}, f32[2048,768]{1,0:T(8,128)}, u32[]{:S(2)}) copy-start(f32[2048,768]{1,0:T(8,128)} %get-tuple-element.238) | copy-start | bytes 18874372 | tf_op jit(solution)/shard_map/while
  119.6 4.6 %copy-start.2 = (f32[2048,768]{1,0:T(8,128)S(1)}, f32[2048,768]{1,0:T(8,128)}, u32[]{:S(2)}) copy-start(f32[2048,768]{1,0:T(8,128)} %get-tuple-element.238) | copy-start | bytes 18874372 | tf_op jit(solution)/shard_map/while
  130.3 4.7 %copy-start.2 = (f32[2048,768]{1,0:T(8,128)S(1)}, f32[2048,768]{1,0:T(8,128)}, u32[]{:S(2)}) copy-start(f32[2048,768]{1,0:T(8,128)} %get-tuple-element.238) | copy-start | bytes 18874372 | tf_op jit(solution)/shard_map/while
  141.0 4.6 %copy-start.2 = (f32[2048,768]{1,0:T(8,128)S(1)}, f32[2048,768]{1,0:T(8,128)}, u32[]{:S(2)}) copy-start(f32[2048,768]{1,0:T(8,128)} %get-tuple-element.238) | copy-start | bytes 18874372 | tf_op jit(solution)/shard_map/while
  147.0 7.4 %copy-start.7 = (bf16[768,256]{1,0:T(8,128)(2,1)S(1)}, bf16[768,256]{1,0:T(8,128)(2,1)}, u32[]{:S(2)}) copy-start(bf16[768,256]{1,0:T(8,128)(2,1)} %param.13) | copy-start | bytes 1179652
  148.6 25.7 %all-to-all-start = ((bf16[8,768,128]{1,2,0:T(8,128)(2,1)}), bf16[8,768,128]{1,2,0:T(8,128)(2,1)S(1)}, u32[]{:S(2)}, u32[]{:S(2)}) async-start(bf16[8,768,128]{1,2,0:T(8,128)(2,1)} %broadcast_in_dim.17), calls=%async_computation | async-start | bytes 3145728 | tf_op jit(solution)/shard_map/all_to_all | solution.py:33
  153.7 89.7 %all-gather.8.cloned.1.call-start = ((), (), s32[]{:S(2)}) async-start(), calls=%async_computation.7 | async-start | bytes 3063808 | tf_op jit(solution)/shard_map/all_gather | solution.py:187
  183.1 10.0 %copy-start.3 = (f32[768,256]{0,1:T(8,128)}, f32[768,256]{0,1:T(8,128)S(1)}, u32[]{:S(2)}) copy-start(f32[768,256]{0,1:T(8,128)S(1)} %get-tuple-element.185) | copy-start | bytes 2359300
  183.7 9.0 %all-to-all-start.2 = ((f32[8,1,768]{2,1,0:T(1,128)}), f32[8,1,768]{2,1,0:T(1,128)S(1)}, u32[]{:S(2)}, u32[]{:S(2)}) async-start(f32[8,1,768]{2,1,0:T(1,128)} %broadcast_in_dim.18), calls=%async_computation.2 | async-start | bytes 49152 | tf_op jit(solution)/shard_map/all_to_all | solution.py:33
  236.6 6.7 %copy-start.5 = (bf16[768,8,256]{0,2,1:T(8,128)(2,1)S(1)}, bf16[768,8,256]{0,2,1:T(8,128)(2,1)}, u32[]{:S(2)}) copy-start(bf16[768,8,256]{0,2,1:T(8,128)(2,1)} %copy.95) | copy-start | bytes 9437188
  256.9 43.2 %copy-start.1 = (bf16[768,256]{1,0:T(8,128)(2,1)S(1)}, bf16[768,256]{1,0:T(8,128)(2,1)}, u32[]{:S(2)}) copy-start(bf16[768,256]{1,0:T(8,128)(2,1)} %param.16) | copy-start | bytes 1179652
  298.0 1.1 copy-start.4
Sparse Core Ops, SparseCore 0:
  13.7 64.4 all-gather.3
  80.3 62.8 all-gather.5
  156.6 48.6 all-gather.7
